TPU v7x, 32 devices: a whole 2x2x4 slice. The times are simulated.
32 devices in a mesh: sp: 4 (over y, x), tp: 8 (over z, core).
Axes of the slice: x: 2, y: 2, z: 4, core: 2. Of those that a mesh axis runs over, the one named last changes fastest.
Arguments:
- cotangent: bfloat16 [1024, 2048], P('sp', 'tp'), may hold values from -6 to 6
- block_input: bfloat16 [1024, 2048], P('sp', 'tp'), may hold values from -6 to 6
- routes: int32 [1024, 2], P('sp'), may hold values from 0 to 3, all different within a row; in each aligned block of 256 rows (0 to 255, 256 to 511, ...) at most 160 rows name the same one
- route_weights: float32 [1024, 2], P('sp'), may hold values from 0.1 to 0.9
- gate_weight: bfloat16 [4, 2048, 7168], P('sp', None, 'tp'), may hold values from -0.125 to 0.125
- up_weight: bfloat16 [4, 2048, 7168], P('sp', None, 'tp'), may hold values from -0.125 to 0.125
- down_weight: bfloat16 [4, 7168, 2048], P('sp', 'tp'), may hold values from -0.0625 to 0.0625
- out_weight: bfloat16 [1024, 2048], P('tp'), may hold values from -0.1875 to 0.1875
- conv_out: bfloat16 [1024, 1024], P('tp', 'sp'), may hold values from -6 to 6
- gate_pre: bfloat16 [1024, 1024], P('tp', 'sp'), may hold values from -6 to 6
- prior_states: bfloat16 [1024, 1024], P('tp', 'sp'), may hold values from -6 to 6
- recur_weight: bfloat16 [16, 64, 64], replicated, may hold values from -0.75 to 0.75
- input_gate_matrix: bfloat16 [16, 64, 64], replicated, may hold values from -0.75 to 0.75
- decay_param: float32 [1024], replicated, may hold values from 4 to 16
- decay_jump: float32 [1024, 1024], P('tp', 'sp'), may hold values from -1 to 0, as said below
Outputs:
- gate_weight_grad: bfloat16 [4, 2048, 7168], P('sp', None, 'tp')
- up_weight_grad: bfloat16 [4, 2048, 7168], P('sp', None, 'tp')
- down_weight_grad: bfloat16 [4, 7168, 2048], P('sp', 'tp')
- out_weight_grad: float32 [1024, 2048], P('tp', 'sp')
- conv_grad: bfloat16 [1024, 1024], P('tp', 'sp')
- valve_logit_derivative: bfloat16 [1024, 1024], P('tp', 'sp')
Inputs may be any that keep to these rules, and one draw needn't show every extreme that they name: In each aligned block of 256 rows (the rows of one index of sp) no expert is named by more than 160 routes, a bound that some block reaches; a row names 2 different experts. `decay_jump`: every entry is at most -1 / 20480.
All inputs are finite; a program needn't handle non-finite values.
Results may differ from a plain program's by a relative error of at most 0.018.
Values may be sent and summed in bfloat16 or wider, within the bound.
A program may use at most 128 MiB of HBM per device.

v0:
```python
import jax
import jax.numpy as jnp
from jax import lax
from jax.sharding import PartitionSpec as P

HEAD_DIM = 64
TOP_K = 2
RATE_SCALE = 8.0


def prefix(value, axis, join, neutral):
    count, mine = (lax.axis_size(axis), lax.axis_index(axis))
    pieces = jax.tree.map(lambda part: lax.all_gather(part, axis), value)
    pieces = jax.tree.map(lambda part: part[::-1], pieces)
    mine = count - 1 - mine
    so_far = jax.tree.map(
        lambda part, zero: jnp.full_like(part, 0) + jnp.asarray(zero, part.dtype), value, neutral
    )

    def turn(position, so_far):
        longer = join(so_far, jax.tree.map(lambda part: part[position], pieces))
        return jax.tree.map(lambda new, old: jnp.where(position < mine, new, old), longer, so_far)

    return lax.fori_loop(0, count - 1, turn, so_far)


def link_pairs(left_pair, right_pair):
    return (left_pair[0] * right_pair[0], right_pair[0] * left_pair[1] + right_pair[1])


def later_first(earlier_pair, later_pair):
    return (earlier_pair[0] * later_pair[0], later_pair[1] + later_pair[0] * earlier_pair[1])


def routing_tables(routes, experts, capacity):
    flat_routes = routes.reshape(-1)
    onehot = (flat_routes[:, None] == jnp.arange(experts, dtype=jnp.int32)[None, :]).astype(
        jnp.int32
    )
    slot_rank = jnp.sum((jnp.cumsum(onehot, axis=0) - onehot) * onehot, axis=1)
    target = (flat_routes * capacity + slot_rank).reshape(routes.shape[0], routes.shape[1])
    slot_ids = jnp.arange(experts * capacity, dtype=jnp.int32)
    return jnp.transpose(target)[:, None, :] == slot_ids[None, :, None]


def spread(placing, route_hits, rows_in, cot_in, route_weights):
    sent_rows = jnp.dot(placing, rows_in, preferred_element_type=jnp.float32).astype(jnp.bfloat16)
    scaled = (
        jnp.transpose(route_weights)[:, :, None] * cot_in.astype(jnp.float32)[None, :, :]
    ).astype(jnp.bfloat16)
    sent_cot = jnp.einsum(
        "kst,ktd->sd", route_hits, scaled, preferred_element_type=jnp.float32
    ).astype(jnp.bfloat16)
    return (sent_rows, sent_cot)


def expert_work(slot_rows, slot_cot, w_gate, w_up, w_down):
    minor = (((1,), (1,)), ((), ()))
    gate_act = jnp.dot(slot_rows, w_gate, preferred_element_type=jnp.float32)
    up_act = jnp.dot(slot_rows, w_up, preferred_element_type=jnp.float32)
    sigma_gate = jax.nn.sigmoid(gate_act)
    silu_val = gate_act * sigma_gate
    hidden = (silu_val * up_act).astype(jnp.bfloat16)
    d_hidden = lax.dot_general(slot_cot, w_down, minor, preferred_element_type=jnp.float32)
    d_gate = (d_hidden * up_act * sigma_gate * (1.0 + gate_act * (1.0 - sigma_gate))).astype(
        jnp.bfloat16
    )
    d_up = (d_hidden * silu_val).astype(jnp.bfloat16)
    width_part = lax.dot_general(d_gate, w_gate, minor, preferred_element_type=jnp.float32)
    width_part = width_part + lax.dot_general(d_up, w_up, minor, preferred_element_type=jnp.float32)
    return (hidden, d_gate, d_up, width_part)


def weight_grads(slot_rows, slot_cot, hidden, d_gate, d_up):
    major = (((0,), (0,)), ((), ()))
    gate_grad = lax.dot_general(
        slot_rows, d_gate, major, preferred_element_type=jnp.float32
    ).astype(jnp.bfloat16)
    up_grad = lax.dot_general(slot_rows, d_up, major, preferred_element_type=jnp.float32).astype(
        jnp.bfloat16
    )
    down_grad = lax.dot_general(hidden, slot_cot, major, preferred_element_type=jnp.float32).astype(
        jnp.bfloat16
    )
    return (gate_grad[None], up_grad[None], down_grad[None])


def local(
    cotangent,
    block_input,
    routes,
    route_weights,
    gate_weight,
    up_weight,
    down_weight,
    out_weight,
    conv_out,
    gate_pre,
    prior_states,
    recur_weight,
    input_gate_matrix,
    decay_param,
    decay_jump,
):
    experts = lax.axis_size("sp")
    tok_rows = cotangent.shape[0]
    capacity = 5 * tok_rows * TOP_K // (4 * experts)
    route_hits = routing_tables(routes, experts, capacity)
    placing = jnp.sum(route_hits.astype(jnp.int32), axis=0).astype(jnp.bfloat16)
    hit_table = route_hits.astype(jnp.bfloat16)
    sent_rows, sent_cot = spread(placing, hit_table, block_input, cotangent, route_weights)
    part_rows, portion_adjoint = (
        lax.all_to_all(
            sent_rows.reshape(experts, capacity, -1), "sp", split_axis=0, concat_axis=0, tiled=True
        ),
        lax.all_to_all(
            sent_cot.reshape(experts, capacity, -1), "sp", split_axis=0, concat_axis=0, tiled=True
        ),
    )
    got_rows, got_cot = (
        lax.all_gather(part_rows, "tp", axis=2, tiled=True),
        lax.all_gather(portion_adjoint, "tp", axis=2, tiled=True),
    )
    full_width = got_rows.shape[2]
    slot_rows = got_rows.reshape(-1, full_width)
    slot_cot = got_cot.reshape(-1, full_width)
    hidden, d_gate, d_up, width_part = expert_work(
        slot_rows, slot_cot, gate_weight[0], up_weight[0], down_weight[0]
    )
    gate_grad, up_grad, down_grad = weight_grads(slot_rows, slot_cot, hidden, d_gate, d_up)
    summed = lax.psum_scatter(
        width_part.reshape(experts, capacity, full_width).astype(jnp.bfloat16),
        "tp",
        scatter_dimension=2,
        tiled=True,
    )
    handed_result = lax.all_to_all(summed, "sp", split_axis=0, concat_axis=0, tiled=True).reshape(
        experts * capacity, -1
    )
    moe_grad = lax.dot_general(
        placing, handed_result, (((0,), (0,)), ((), ())), preferred_element_type=jnp.float32
    )
    block_grad = (cotangent.astype(jnp.float32) + moe_grad).astype(jnp.bfloat16)
    full_grad = lax.all_gather(block_grad, "tp", axis=1, tiled=True)
    channels = conv_out.shape[0]
    length = conv_out.shape[1]
    head_count = channels // HEAD_DIM
    head_start = lax.axis_index("tp") * head_count
    w_recur = lax.dynamic_slice_in_dim(recur_weight, head_start, head_count, 0)
    w_input = lax.dynamic_slice_in_dim(input_gate_matrix, head_start, head_count, 0)
    rate_parameter = lax.dynamic_slice_in_dim(decay_param, head_start * HEAD_DIM, channels, 0)[
        :, None
    ]
    shaped = conv_out.reshape(head_count, HEAD_DIM, length)
    recur_gate = jax.nn.sigmoid(
        jnp.einsum("hij,hit->hjt", w_recur, shaped, preferred_element_type=jnp.float32).reshape(
            channels, length
        )
    )
    input_gate = jax.nn.sigmoid(
        jnp.einsum("hij,hit->hjt", w_input, shaped, preferred_element_type=jnp.float32).reshape(
            channels, length
        )
    )
    softened = jax.nn.softplus(-rate_parameter)
    log_decay = -RATE_SCALE * recur_gate * softened + decay_jump
    decay_val = jnp.exp(log_decay)
    norm_scale = jnp.sqrt(-jnp.expm1(2.0 * log_decay))
    conv_vals = conv_out.astype(jnp.float32)
    prior_vals = prior_states.astype(jnp.float32)
    state = decay_val * prior_vals + norm_scale * input_gate * conv_vals
    gelu_val, gelu_pull = jax.vjp(jax.nn.gelu, gate_pre.astype(jnp.float32))
    mixed = (gelu_val * state).astype(jnp.bfloat16)
    d_mixed = lax.dot_general(
        out_weight, full_grad, (((1,), (1,)), ((), ())), preferred_element_type=jnp.float32
    )
    valve_logit_derivative = gelu_pull(d_mixed * state)[0].astype(jnp.bfloat16)
    d_state = d_mixed * gelu_val
    shifted = jnp.concatenate([decay_val[:, 1:], jnp.ones((channels, 1), jnp.float32)], axis=1)
    flipped = lax.associative_scan(link_pairs, (jnp.flip(shifted, 1), jnp.flip(d_state, 1)), axis=1)
    decay_prod = jnp.flip(flipped[0], 1)
    local_sum = jnp.flip(flipped[1], 1)
    summary = (decay_val[:, 0] * decay_prod[:, 0], decay_val[:, 0] * local_sum[:, 0])
    carried = prefix(
        summary,
        "sp",
        later_first,
        (jnp.ones((channels,), jnp.float32), jnp.zeros((channels,), jnp.float32)),
    )[1]
    state_grad = local_sum + decay_prod * carried[:, None]
    grad_log = (
        state_grad * prior_vals * decay_val
        - state_grad * input_gate * conv_vals * decay_val * decay_val / norm_scale
    )
    grad_recur = (grad_log * -RATE_SCALE * softened * recur_gate * (1.0 - recur_gate)).astype(
        jnp.bfloat16
    )
    grad_input = (state_grad * norm_scale * conv_vals * input_gate * (1.0 - input_gate)).astype(
        jnp.bfloat16
    )
    back_recur = jnp.einsum(
        "hij,hjt->hit",
        w_recur,
        grad_recur.reshape(head_count, HEAD_DIM, length),
        preferred_element_type=jnp.float32,
    ).reshape(channels, length)
    back_input = jnp.einsum(
        "hij,hjt->hit",
        w_input,
        grad_input.reshape(head_count, HEAD_DIM, length),
        preferred_element_type=jnp.float32,
    ).reshape(channels, length)
    conv_grad = (state_grad * norm_scale * input_gate + back_recur + back_input).astype(
        jnp.bfloat16
    )
    projected = lax.psum_scatter(
        lax.dot_general(
            full_grad, mixed, (((0,), (1,)), ((), ())), preferred_element_type=jnp.float32
        ).astype(jnp.bfloat16),
        "sp",
        scatter_dimension=0,
        tiled=True,
    ).astype(jnp.float32)
    out_weight_grad = jnp.transpose(projected)
    return (gate_grad, up_grad, down_grad, out_weight_grad, conv_grad, valve_logit_derivative)


def solution(mesh):
    in_specs = (
        P("sp", "tp"),
        P("sp", "tp"),
        P("sp", None),
        P("sp", None),
        P("sp", None, "tp"),
        P("sp", None, "tp"),
        P("sp", "tp", None),
        P("tp", None),
        P("tp", "sp"),
        P("tp", "sp"),
        P("tp", "sp"),
        P(),
        P(),
        P(),
        P("tp", "sp"),
    )
    out_specs = (
        P("sp", None, "tp"),
        P("sp", None, "tp"),
        P("sp", "tp", None),
        P("tp", "sp"),
        P("tp", "sp"),
        P("tp", "sp"),
    )
    return jax.shard_map(local, mesh=mesh, in_specs=in_specs, out_specs=out_specs, check_vma=False)
```

profile of v0, /device:TPU:0, one launch (start us, length us, event | category | flops | bytes accessed | tf_op | source)
XLA Modules:
  0.0 229.2 jit_solution(16892057116044407689)
XLA Ops:
  7.2 0.9 copy.72
  8.1 0.1 eq.42
  8.3 0.1 eq.38
  8.4 1.2 reduce-window.6
  9.7 0.2 slice_reduce_fusion
  9.9 0.2 reduce-window.9
  10.2 0.1 reduce_sum.21
  10.4 0.7 add_bitcast_fusion.1
  11.1 0.3 convert_reduce_fusion
  11.3 1.1 convolution_convert_fusion.1
  12.5 11.7 %all_to_all.15 = bf16[4,160,256]{2,1,0:T(8,128)(2,1)} all-to-all(bf16[4,160,256]{2,1,0:T(8,128)(2,1)S(1)} %bitcast.101), channel_id=1, replica_groups=mesh['sp'=4,'tp'=8] {'sp'}, dimensions={0} | all-to-all | bytes 655360 | tf_op jit(solution)/shard_map/all_to_all | solution.py:113
  24.3 0.5 fusion.16
  24.8 9.3 %all_to_all.16 = bf16[4,160,256]{2,1,0:T(8,128)(2,1)} all-to-all(bf16[4,160,256]{2,1,0:T(8,128)(2,1)S(1)} %bitcast.104), channel_id=1, replica_groups=mesh['sp'=4,'tp'=8] {'sp'}, dimensions={0} | all-to-all | bytes 655360 | tf_op jit(solution)/shard_map/all_to_all | solution.py:116
  34.2 24.6 %all-gather.6.cloned.1.call-done = bf16[4,160,2048]{2,1,0:T(8,128)(2,1)} async-done(((bf16[4,160,256]{2,1,0:T(8,128)(2,1)}), bf16[4,160,2048]{2,1,0:T(8,128)(2,1)}) %all-gather.6.cloned.1.call-update) | async-done | bytes 2621456 | tf_op jit(solution)/shard_map/all_gather | solution.py:121
  58.8 7.2 %fusion.3 = f32[640,896]{1,0:T(8,128)} fusion(bf16[640,2048]{1,0:T(8,128)(2,1)} %bitcast.114, bf16[1,2048,896]{2,1,0:T(8,128)(2,1)} %param.21), kind=kOutput, calls=%fused_computation.7 | convolution fusion | flops 2348810240 | bytes 8585216 | tf_op jit(solution)/shard_map/dot_general | solution.py:59
  66.0 4.3 %fusion.7 = f32[640,896]{1,0:T(8,128)} fusion(bf16[640,2048]{1,0:T(8,128)(2,1)S(1)} %bitcast.116, bf16[1,2048,896]{2,1,0:T(8,128)(2,1)S(1)} %copy-done.8), kind=kOutput, calls=%fused_computation.11 | convolution fusion | flops 2348810240 | bytes 8585216 | tf_op jit(solution)/shard_map/dot_general | solution.py:60
  70.4 23.2 %all-gather.8.cloned.1.call-done = bf16[4,160,2048]{2,1,0:T(8,128)(2,1)} async-done(((bf16[4,160,256]{2,1,0:T(8,128)(2,1)}), bf16[4,160,2048]{2,1,0:T(8,128)(2,1)}) %all-gather.8.cloned.1.call-update) | async-done | bytes 2621456 | tf_op jit(solution)/shard_map/all_gather | solution.py:122
  93.6 7.8 %multiply_convert_fusion.1 = (bf16[640,896]{1,0:T(8,128)(2,1)S(1)}, bf16[640,896]{1,0:T(8,128)(2,1)S(1)}) fusion(f32[640,896]{1,0:T(8,128)} %fusion.3, f32[640,896]{1,0:T(8,128)} %fusion.7, bf16[640,2048]{1,0:T(8,128)(2,1)} %bitcast.118, bf16[1,896,2048]{2,1,0:T(8,128)(2,1)} %param.23), kind=kOutput, calls=%fused_computation.20 | convolution fusion | flops 2356264960 | bytes 13172736 | tf_op jit(solution)/shard_map/dot_general | solution.py:64
  101.5 2.9 %fusion.1 = f32[640,2048]{1,0:T(8,128)S(1)} fusion(bf16[640,896]{1,0:T(8,128)(2,1)S(1)} %get-tuple-element.152, bf16[1,2048,896]{2,1,0:T(8,128)(2,1)S(1)} %copy-done.7), kind=kOutput, calls=%fused_computation.5 | convolution fusion | flops 2348810240 | bytes 10059776 | tf_op jit(solution)/shard_map/dot_general | solution.py:69
  104.4 4.2 %add_convert_fusion = bf16[640,2048]{1,0:T(8,128)(2,1)} fusion(f32[640,2048]{1,0:T(8,128)S(1)} %fusion.1, bf16[640,896]{1,0:T(8,128)(2,1)S(1)} %get-tuple-element.151, bf16[1,2048,896]{2,1,0:T(8,128)(2,1)S(1)} %copy-done.9), kind=kOutput, calls=%fused_computation.4 | convolution fusion | flops 2351431680 | bytes 12681216 | tf_op jit(solution)/shard_map/dot_general | solution.py:70
  108.6 0.8 copy-done.4
  109.5 1.0 fusion.23
  110.7 34.2 %reduce-scatter.3.cloned.1.call-done = bf16[4,160,256]{2,1,0:T(8,128)(2,1)} async-done(((bf16[4,160,2048]{2,1,0:T(8,128)(2,1)}), bf16[4,160,256]{2,1,0:T(8,128)(2,1)}) %reduce-scatter.3.cloned.1.call-update) | async-done | bytes 327696 | tf_op jit(solution)/shard_map/reduce_scatter | solution.py:131
  144.9 3.7 %all-to-all-start.2 = ((bf16[4,160,256]{2,1,0:T(8,128)(2,1)}), bf16[4,160,256]{2,1,0:T(8,128)(2,1)S(1)}, u32[]{:S(2)}, u32[]{:S(2)}) async-start(bf16[4,160,256]{2,1,0:T(8,128)(2,1)} %reduce-scatter.3.cloned.1.call-done), calls=%async_computation.3 | async-start | bytes 655360 | tf_op jit(solution)/shard_map/all_to_all | solution.py:137
  148.6 1.0 fusion.21
  149.7 0.1 copy.79
  149.8 0.1 copy.75
  150.0 0.8 fusion.70
  150.8 3.3 %all-to-all-done.2 = bf16[4,160,256]{2,1,0:T(8,128)(2,1)S(1)} async-done(((bf16[4,160,256]{2,1,0:T(8,128)(2,1)}), bf16[4,160,256]{2,1,0:T(8,128)(2,1)S(1)}, u32[]{:S(2)}, u32[]{:S(2)}) %all-to-all-start.2) | async-done | bytes 327712 | tf_op jit(solution)/shard_map/all_to_all | solution.py:137
  154.1 1.0 fusion.17
  155.1 7.4 %convert_bitcast_fusion.1 = bf16[1,2048,896]{2,1,0:T(8,128)(2,1)} fusion(bf16[640,2048]{1,0:T(8,128)(2,1)} %bitcast.115, bf16[640,896]{1,0:T(8,128)(2,1)} %copy-done.18), kind=kOutput, calls=%fused_computation.16 | convolution fusion | flops 2350645248 | bytes 7438336 | tf_op jit(solution)/shard_map/dot_general | solution.py:79
  162.6 4.9 %convert_bitcast_fusion.2 = bf16[1,2048,896]{2,1,0:T(8,128)(2,1)} fusion(bf16[640,2048]{1,0:T(8,128)(2,1)S(1)} %bitcast.117, bf16[640,896]{1,0:T(8,128)(2,1)S(1)} %copy-done.15), kind=kOutput, calls=%fused_computation.17 | convolution fusion | flops 2350645248 | bytes 7438336 | tf_op jit(solution)/shard_map/dot_general | solution.py:76
  167.5 4.6 %convert_bitcast_fusion = bf16[1,896,2048]{2,1,0:T(8,128)(2,1)} fusion(bf16[640,2048]{1,0:T(8,128)(2,1)S(1)} %bitcast.119, f32[640,896]{1,0:T(8,128)S(1)} %copy-done.17, f32[640,896]{1,0:T(8,128)S(1)} %copy-done.16), kind=kOutput, calls=%fused_computation.15 | convolution fusion | flops 2354085888 | bytes 10878976 | tf_op jit(solution)/shard_map/dot_general | solution.py:82
  172.1 4.3 %all-gather.10.cloned.1.call-done = bf16[256,2048]{1,0:T(8,128)(2,1)} async-done(((bf16[256,256]{1,0:T(8,128)(2,1)}), bf16[256,2048]{1,0:T(8,128)(2,1)}) %all-gather.10.cloned.1.call-update) | async-done | bytes 1048592 | tf_op jit(solution)/shard_map/all_gather | solution.py:144
  176.4 1.7 fusion.40
  180.3 7.2 %all-gather = f32[512,1]{0,1:T(1,128)S(1)} all-gather(f32[128,1]{0,1:T(1,128)S(1)} %get-tuple-element.156), channel_id=2, replica_groups=mesh['sp'=4,'tp'=8] {'sp'}, dimensions={0}, use_global_device_ids=true | all-gather | bytes 2560 | tf_op jit(solution)/shard_map/all_gather | solution.py:13
  187.5 7.9 %all-gather.1 = f32[512,1]{0,1:T(1,128)S(1)} all-gather(f32[128,1]{0,1:T(1,128)S(1)} %get-tuple-element.155), channel_id=3, replica_groups=mesh['sp'=4,'tp'=8] {'sp'}, dimensions={0}, use_global_device_ids=true | all-gather | bytes 2560 | tf_op jit(solution)/shard_map/all_gather | solution.py:13
  195.4 1.4 convolution_convert_fusion
  196.8 0.1 while.14
  197.2 0.2 fusion.43
  197.5 0.9 fusion.62
  198.5 0.1 copy.92
  198.6 0.9 fusion.59
  199.7 0.7 copy.96
  200.4 0.7 copy.97
  201.1 19.8 %reduce-scatter.5.cloned.1.call-done = bf16[512,128]{1,0:T(8,128)(2,1)} async-done(((bf16[2048,128]{1,0:T(8,128)(2,1)}), bf16[512,128]{1,0:T(8,128)(2,1)}) %reduce-scatter.5.cloned.1.call-update) | async-done | bytes 131088 | tf_op jit(solution)/shard_map/reduce_scatter | solution.py:216
  220.9 0.9 convert_bitcast_fusion.3
  221.8 0.8 copy.95
  (201 shorter events, 3.0 us)
Async XLA Ops:
  7.2 169.2 %copy-start = (bf16[128,2048]{1,0:T(8,128)(2,1)S(1)}, bf16[128,2048]{1,0:T(8,128)(2,1)}, u32[]{:S(2)}) copy-start(bf16[128,2048]{1,0:T(8,128)(2,1)} %param.24) | copy-start | bytes 1572868
  7.2 17.1 %copy-start.2 = (bf16[256,256]{1,0:T(8,128)(2,1)S(1)}, bf16[256,256]{1,0:T(8,128)(2,1)}, u32[]{:S(2)}) copy-start(bf16[256,256]{1,0:T(8,128)(2,1)} %param.17) | copy-start | bytes 393220
  7.2 17.1 %copy-start.13 = (f32[256,2]{0,1:T(2,128)S(1)}, f32[256,2]{0,1:T(2,128)}, u32[]{:S(2)}) copy-start(f32[256,2]{0,1:T(2,128)} %param.20) | copy-start | bytes 6148
  7.2 51.6 %all-gather.6.cloned.1.call-start = ((), (), s32[]{:S(2)}) async-start(), calls=%async_computation.5 | async-start | bytes 2949120 | tf_op jit(solution)/shard_map/all_gather | solution.py:121
  24.2 69.4 %all-gather.8.cloned.1.call-start = ((), (), s32[]{:S(2)}) async-start(), calls=%async_computation.6 | async-start | bytes 2949120 | tf_op jit(solution)/shard_map/all_gather | solution.py:122
  34.1 110.8 %reduce-scatter.3.cloned.1.call-start = ((), (), s32[]{:S(2)}) async-start(), calls=%async_computation.7 | async-start | bytes 2949120 | tf_op jit(solution)/shard_map/reduce_scatter | solution.py:131
  58.8 7.2 %copy-start.8 = (bf16[1,2048,896]{2,1,0:T(8,128)(2,1)S(1)}, bf16[1,2048,896]{2,1,0:T(8,128)(2,1)}, u32[]{:S(2)}) copy-start(bf16[1,2048,896]{2,1,0:T(8,128)(2,1)} %param.22) | copy-start | bytes 11010052
  58.8 7.2 %copy-start.10 = (bf16[4,160,2048]{2,1,0:T(8,128)(2,1)S(1)}, bf16[4,160,2048]{2,1,0:T(8,128)(2,1)}, u32[]{:S(2)}) copy-start(bf16[4,160,2048]{2,1,0:T(8,128)(2,1)} %all-gather.6.cloned.1.call-done) | copy-start | bytes 7864324
  93.6 7.8 %copy-start.7 = (bf16[1,2048,896]{2,1,0:T(8,128)(2,1)S(1)}, bf16[1,2048,896]{2,1,0:T(8,128)(2,1)}, u32[]{:S(2)}) copy-start(bf16[1,2048,896]{2,1,0:T(8,128)(2,1)} %param.21) | copy-start | bytes 11010052
  101.4 3.0 %copy-start.14 = (bf16[640,896]{1,0:T(8,128)(2,1)}, bf16[640,896]{1,0:T(8,128)(2,1)S(1)}, u32[]{:S(2)}) copy-start(bf16[640,896]{1,0:T(8,128)(2,1)S(1)} %get-tuple-element.152) | copy-start | bytes 3440644
  101.4 3.0 %copy-start.18 = (bf16[640,896]{1,0:T(8,128)(2,1)}, bf16[640,896]{1,0:T(8,128)(2,1)S(1)}, u32[]{:S(2)}) copy-start(bf16[640,896]{1,0:T(8,128)(2,1)S(1)} %get-tuple-element.151) | copy-start | bytes 3440644
  101.4 2.9 %copy-start.9 = (bf16[1,2048,896]{2,1,0:T(8,128)(2,1)S(1)}, bf16[1,2048,896]{2,1,0:T(8,128)(2,1)}, u32[]{:S(2)}) copy-start(bf16[1,2048,896]{2,1,0:T(8,128)(2,1)} %param.22) | copy-start | bytes 11010052
  108.6 0.8 copy-start.4
  108.6 41.1 %copy-start.5 = (bf16[128,256]{1,0:T(8,128)(2,1)S(1)}, bf16[128,256]{1,0:T(8,128)(2,1)}, u32[]{:S(2)}) copy-start(bf16[128,256]{1,0:T(8,128)(2,1)} %param.27) | copy-start | bytes 196612
  108.6 41.2 %copy-start.6 = (bf16[128,256]{1,0:T(8,128)(2,1)S(1)}, bf16[128,256]{1,0:T(8,128)(2,1)}, u32[]{:S(2)}) copy-start(bf16[128,256]{1,0:T(8,128)(2,1)} %param.26) | copy-start | bytes 196612
  108.6 41.3 %copy-start.3 = (f32[128,256]{1,0:T(8,128)S(1)}, f32[128,256]{1,0:T(8,128)}, u32[]{:S(2)}) copy-start(f32[128,256]{1,0:T(8,128)} %param.31) | copy-start | bytes 393220
  144.9 9.2 %all-to-all-start.2 = ((bf16[4,160,256]{2,1,0:T(8,128)(2,1)}), bf16[4,160,256]{2,1,0:T(8,128)(2,1)S(1)}, u32[]{:S(2)}, u32[]{:S(2)}) async-start(bf16[4,160,256]{2,1,0:T(8,128)(2,1)} %reduce-scatter.3.cloned.1.call-done), calls=%async_computation.3 | async-start | bytes 655360 | tf_op jit(solution)/shard_map/all_to_all | solution.py:137
  148.5 27.9 %all-gather.10.cloned.1.call-start = ((), (), s32[]{:S(2)}) async-start(), calls=%async_computation.8 | async-start | bytes 1179648 | tf_op jit(solution)/shard_map/all_gather | solution.py:144
  155.1 7.5 %copy-start.15 = (bf16[640,896]{1,0:T(8,128)(2,1)S(1)}, bf16[640,896]{1,0:T(8,128)(2,1)}, u32[]{:S(2)}) copy-start(bf16[640,896]{1,0:T(8,128)(2,1)} %copy-done.14) | copy-start | bytes 3440644
  155.1 65.8 %reduce-scatter.5.cloned.1.call-start = ((), (), s32[]{:S(2)}) async-start(), calls=%async_computation.9 | async-start | bytes 655360 | tf_op jit(solution)/shard_map/reduce_scatter | solution.py:216
  155.1 7.4 %copy-start.11 = (bf16[4,160,2048]{2,1,0:T(8,128)(2,1)S(1)}, bf16[4,160,2048]{2,1,0:T(8,128)(2,1)}, u32[]{:S(2)}) copy-start(bf16[4,160,2048]{2,1,0:T(8,128)(2,1)} %all-gather.6.cloned.1.call-done) | copy-start | bytes 7864324
  162.5 4.9 %copy-start.12 = (bf16[4,160,2048]{2,1,0:T(8,128)(2,1)S(1)}, bf16[4,160,2048]{2,1,0:T(8,128)(2,1)}, u32[]{:S(2)}) copy-start(bf16[4,160,2048]{2,1,0:T(8,128)(2,1)} %all-gather.8.cloned.1.call-done) | copy-start | bytes 7864324
  162.5 4.9 %copy-start.16 = (f32[640,896]{1,0:T(8,128)S(1)}, f32[640,896]{1,0:T(8,128)}, u32[]{:S(2)}) copy-start(f32[640,896]{1,0:T(8,128)} %fusion.3) | copy-start | bytes 6881284
  162.6 4.9 %copy-start.17 = (f32[640,896]{1,0:T(8,128)S(1)}, f32[640,896]{1,0:T(8,128)}, u32[]{:S(2)}) copy-start(f32[640,896]{1,0:T(8,128)} %fusion.7) | copy-start | bytes 6881284
  178.5 16.9 %copy-start.1 = (bf16[256,2048]{1,0:T(8,128)(2,1)S(1)}, bf16[256,2048]{1,0:T(8,128)(2,1)}, u32[]{:S(2)}) copy-start(bf16[256,2048]{1,0:T(8,128)(2,1)} %all-gather.10.cloned.1.call-done) | copy-start | bytes 3145732
Sparse Core Ops, SparseCore 0:
  24.3 34.4 all-gather.5
  60.4 33.1 all-gather.7
  108.7 36.0 reduce-scatter.2
  155.2 21.1 all-gather.9
  196.9 23.9 reduce-scatter.4
where the time goes:
time: 230 us; the launch traced here: 229 us
  waiting for transfers between devices  110 us (48%)
  matrix products  52.8 us (23%)
  blocking collectives  36 us (16%)
  between operations  14.9 us (6%)
  local copies, waits for them, and re-layouts  7.07 us (3%)
  other arithmetic  4.91 us (2%)
  starting transfers between devices  3.85 us (2%)
    reduce_scatter x1, waiting for transfers between devices, local(): lax.psum_scatter(width_part.reshape(experts, capacity, full_width).astype...  34.2 us
    all_gather x1, waiting for transfers between devices, local(): lax.all_gather(part_rows, 'tp', axis=2, tiled=True)  24.6 us
    all_gather x1, waiting for transfers between devices, local(): lax.all_gather(portion_adjoint, 'tp', axis=2, tiled=True)  23.2 us
    reduce_scatter x1, waiting for transfers between devices, local(): lax.psum_scatter(lax.dot_general(full_grad, mixed, (((0,), (1,)), ((), ()...  19.8 us
    all_gather x2, blocking collectives, prefix(): pieces = jax.tree.map(lambda part: lax.all_gather(part, axis), value)  15 us
    all_to_all x1, blocking collectives, local(): lax.all_to_all(sent_rows.reshape(experts, capacity, -1), 'sp', split_axis...  11.7 us
    all_to_all x1, blocking collectives, local(): lax.all_to_all(sent_cot.reshape(experts, capacity, -1), 'sp', split_axis=...  9.32 us
    dot_general x1, matrix products, expert_work(): lax.dot_general(slot_cot, w_down, minor, preferred_element_type=jnp.float32)  7.79 us
  transfers between devices with their start and end apart: 6, of which 6 were waited for; matrix products, arithmetic and copies ran while one was open for 16% of the time, Pallas kernels for 0%

commit v1 on v0

--- a/solution.py
+++ b/solution.py
@@ -2,6 +2,7 @@
 import jax.numpy as jnp
 from jax import lax
 from jax.sharding import PartitionSpec as P
+from jax.lax import all_gather
 
 HEAD_DIM = 64
 TOP_K = 2
@@ -117,8 +118,11 @@
             sent_cot.reshape(experts, capacity, -1), "sp", split_axis=0, concat_axis=0, tiled=True
         ),
     )
+    pair_the_meshes = lambda base_x, mesh_ax: jnp.concatenate(
+        all_gather(base_x, axis_name=mesh_ax), 2
+    )
     got_rows, got_cot = (
-        lax.all_gather(part_rows, "tp", axis=2, tiled=True),
+        pair_the_meshes(part_rows, "tp"),
         lax.all_gather(portion_adjoint, "tp", axis=2, tiled=True),
     )
     full_width = got_rows.shape[2]

time: 230 us -> 230 us (level)
  local copies, waits for them, and re-layouts: 7.07 us -> 14.7 us
  waiting for transfers between devices: 110 us -> 105 us
  matrix products: 52.8 us -> 50 us
    unnamed x46 -> x55, local copies, waits for them, and re-layouts: 4.49 us -> 8.28 us
    reshape x0 -> x1, local copies, waits for them, and re-layouts: none -> 3.23 us  [local(): jnp.concatenate(all_gather(base_x, axis_name=mesh_ax), 2)]
    dot_general x1, matrix products: 7.21 us -> 4.3 us  [expert_work(): gate_act = jnp.dot(slot_rows, w_gate, preferred_element_type=jnp.float32)]
  transfers between devices with their start and end apart: 6 -> 6, of which waited for: 6 -> 6; matrix products, arithmetic and copies ran while one was open for 16% -> 17% of each run, Pallas kernels for 0% -> 0%
where the time goes in v1:
time: 230 us
  waiting for transfers between devices  105 us (46%)
  matrix products  50 us (22%)
  blocking collectives  36.1 us (16%)
  between operations  14.9 us (6%)
  local copies, waits for them, and re-layouts  14.7 us (6%)
  other arithmetic  4.89 us (2%)
  starting transfers between devices  3.79 us (2%)
    reduce_scatter x1, waiting for transfers between devices, local(): lax.psum_scatter(width_part.reshape(experts, capacity, full_width).astype...  34.3 us
    all_gather x1, waiting for transfers between devices, local(): all_gather(base_x, axis_name=mesh_ax)  23.4 us
    all_gather x1, waiting for transfers between devices, local(): lax.all_gather(portion_adjoint, 'tp', axis=2, tiled=True)  21.3 us
    reduce_scatter x1, waiting for transfers between devices, local(): lax.psum_scatter(lax.dot_general(full_grad, mixed, (((0,), (1,)), ((), ()...  19.8 us
    all_gather x2, blocking collectives, prefix(): pieces = jax.tree.map(lambda part: lax.all_gather(part, axis), value)  15 us
    all_to_all x1, blocking collectives, local(): lax.all_to_all(sent_rows.reshape(experts, capacity, -1), 'sp', split_axis...  11.7 us
    all_to_all x1, blocking collectives, local(): lax.all_to_all(sent_cot.reshape(experts, capacity, -1), 'sp', split_axis=...  9.32 us
    unnamed x55, local copies, waits for them, and re-layouts  8.28 us
  transfers between devices with their start and end apart: 6, of which 6 were waited for; matrix products, arithmetic and copies ran while one was open for 17% of the time, Pallas kernels for 0%

profile of v1, /device:TPU:0, one launch (start us, length us, event | category | flops | bytes accessed | tf_op | source)
XLA Modules:
  0.0 229.5 jit_solution(11845344176852068890)
XLA Ops:
  7.2 0.9 copy.130
  8.1 0.1 eq.42
  8.4 1.2 reduce-window.6
  9.7 0.2 slice_reduce_fusion
  9.9 0.2 reduce-window.9
  10.4 0.7 add_bitcast_fusion.1
  11.1 0.3 convert_reduce_fusion
  11.3 1.1 convolution_convert_fusion.1
  12.5 11.7 %all_to_all.15 = bf16[4,160,256]{2,1,0:T(8,128)(2,1)} all-to-all(bf16[4,160,256]{2,1,0:T(8,128)(2,1)S(1)} %bitcast.112), channel_id=1, replica_groups=mesh['sp'=4,'tp'=8] {'sp'}, dimensions={0} | all-to-all | bytes 655360 | tf_op jit(solution)/shard_map/all_to_all | solution.py:114
  24.3 0.5 fusion.16
  24.8 9.3 %all_to_all.16 = bf16[4,160,256]{2,1,0:T(8,128)(2,1)} all-to-all(bf16[4,160,256]{2,1,0:T(8,128)(2,1)S(1)} %bitcast.115), channel_id=1, replica_groups=mesh['sp'=4,'tp'=8] {'sp'}, dimensions={0} | all-to-all | bytes 655360 | tf_op jit(solution)/shard_map/all_to_all | solution.py:117
  34.2 23.4 %all-gather.11.cloned.1.call-done = bf16[32,160,256]{2,1,0:T(8,128)(2,1)} async-done(((bf16[4,160,256]{2,1,0:T(8,128)(2,1)}), bf16[32,160,256]{2,1,0:T(8,128)(2,1)}) %all-gather.11.cloned.1.call-update) | async-done | bytes 2621456 | tf_op jit(solution)/shard_map/all_gather | solution.py:122
  57.6 3.2 %copy.133 = bf16[4,160,8,256]{3,2,1,0:T(8,128)(2,1)S(1)} copy(bf16[4,160,8,256]{3,1,0,2:T(8,128)(2,1)} %bitcast.110) | data formatting | bytes 5242880 | tf_op jit(solution)/shard_map/reshape | solution.py:121
  60.9 0.9 copy.162
  61.8 1.6 copy-done.12
  63.4 4.3 %fusion.3 = f32[640,896]{1,0:T(8,128)} fusion(bf16[640,2048]{1,0:T(8,128)(2,1)S(1)} %bitcast.105, bf16[1,2048,896]{2,1,0:T(8,128)(2,1)S(1)} %copy-done.12), kind=kOutput, calls=%fused_computation.7 | convolution fusion | flops 2348810240 | bytes 8585216 | tf_op jit(solution)/shard_map/dot_general | solution.py:60
  67.7 4.3 %fusion.7 = f32[640,896]{1,0:T(8,128)} fusion(bf16[640,2048]{1,0:T(8,128)(2,1)S(1)} %bitcast.106, bf16[1,2048,896]{2,1,0:T(8,128)(2,1)S(1)} %copy-done.14), kind=kOutput, calls=%fused_computation.11 | convolution fusion | flops 2348810240 | bytes 8585216 | tf_op jit(solution)/shard_map/dot_general | solution.py:61
  71.9 21.3 %all-gather.7.cloned.1.call-done = bf16[4,160,2048]{2,1,0:T(8,128)(2,1)} async-done(((bf16[4,160,256]{2,1,0:T(8,128)(2,1)}), bf16[4,160,2048]{2,1,0:T(8,128)(2,1)}) %all-gather.7.cloned.1.call-update) | async-done | bytes 2621456 | tf_op jit(solution)/shard_map/all_gather | solution.py:126
  93.3 7.8 %multiply_convert_fusion.1 = (bf16[640,896]{1,0:T(8,128)(2,1)S(1)}, bf16[640,896]{1,0:T(8,128)(2,1)S(1)}) fusion(f32[640,896]{1,0:T(8,128)} %fusion.3, f32[640,896]{1,0:T(8,128)} %fusion.7, bf16[640,2048]{1,0:T(8,128)(2,1)} %bitcast.125, bf16[1,896,2048]{2,1,0:T(8,128)(2,1)} %param.23), kind=kOutput, calls=%fused_computation.20 | convolution fusion | flops 2356264960 | bytes 13172736 | tf_op jit(solution)/shard_map/dot_general | solution.py:65
  101.1 2.9 %fusion.1 = f32[640,2048]{1,0:T(8,128)S(1)} fusion(bf16[640,896]{1,0:T(8,128)(2,1)S(1)} %get-tuple-element.164, bf16[1,2048,896]{2,1,0:T(8,128)(2,1)S(1)} %copy-done.13), kind=kOutput, calls=%fused_computation.5 | convolution fusion | flops 2348810240 | bytes 10059776 | tf_op jit(solution)/shard_map/dot_general | solution.py:70
  104.0 4.4 %add_convert_fusion = bf16[640,2048]{1,0:T(8,128)(2,1)} fusion(f32[640,2048]{1,0:T(8,128)S(1)} %fusion.1, bf16[640,896]{1,0:T(8,128)(2,1)S(1)} %get-tuple-element.163, bf16[1,2048,896]{2,1,0:T(8,128)(2,1)S(1)} %copy-done.15), kind=kOutput, calls=%fused_computation.4 | convolution fusion | flops 2351431680 | bytes 12681216 | tf_op jit(solution)/shard_map/dot_general | solution.py:71
  108.5 0.8 copy-done.9
  109.4 1.0 fusion.23
  110.5 34.3 %reduce-scatter.3.cloned.1.call-done = bf16[4,160,256]{2,1,0:T(8,128)(2,1)} async-done(((bf16[4,160,2048]{2,1,0:T(8,128)(2,1)}), bf16[4,160,256]{2,1,0:T(8,128)(2,1)}) %reduce-scatter.3.cloned.1.call-update) | async-done | bytes 327696 | tf_op jit(solution)/shard_map/reduce_scatter | solution.py:135
  144.7 3.6 %all-to-all-start.2 = ((bf16[4,160,256]{2,1,0:T(8,128)(2,1)}), bf16[4,160,256]{2,1,0:T(8,128)(2,1)S(1)}, u32[]{:S(2)}, u32[]{:S(2)}) async-start(bf16[4,160,256]{2,1,0:T(8,128)(2,1)} %reduce-scatter.3.cloned.1.call-done), calls=%async_computation.3 | async-start | bytes 655360 | tf_op jit(solution)/shard_map/all_to_all | solution.py:141
  148.4 1.0 fusion.21
  149.4 0.7 copy.136
  150.2 0.7 copy.134
  151.0 0.7 copy.137
  151.7 0.8 fusion.70
  152.5 1.4 all-to-all-done.2
  153.9 1.0 fusion.17
  155.0 7.4 %convert_bitcast_fusion.1 = bf16[1,2048,896]{2,1,0:T(8,128)(2,1)} fusion(bf16[640,2048]{1,0:T(8,128)(2,1)} %bitcast.107, bf16[640,896]{1,0:T(8,128)(2,1)} %copy-done.22), kind=kOutput, calls=%fused_computation.16 | convolution fusion | flops 2350645248 | bytes 7438336 | tf_op jit(solution)/shard_map/dot_general | solution.py:80
  162.4 4.8 %convert_bitcast_fusion.2 = bf16[1,2048,896]{2,1,0:T(8,128)(2,1)} fusion(bf16[640,2048]{1,0:T(8,128)(2,1)S(1)} %bitcast.108, bf16[640,896]{1,0:T(8,128)(2,1)S(1)} %copy-done.19), kind=kOutput, calls=%fused_computation.17 | convolution fusion | flops 2350645248 | bytes 7438336 | tf_op jit(solution)/shard_map/dot_general | solution.py:77
  167.3 4.6 %convert_bitcast_fusion = bf16[1,896,2048]{2,1,0:T(8,128)(2,1)} fusion(bf16[640,2048]{1,0:T(8,128)(2,1)S(1)} %bitcast.126, f32[640,896]{1,0:T(8,128)S(1)} %copy-done.21, f32[640,896]{1,0:T(8,128)S(1)} %copy-done.20), kind=kOutput, calls=%fused_computation.15 | convolution fusion | flops 2354085888 | bytes 10878976 | tf_op jit(solution)/shard_map/dot_general | solution.py:83
  171.9 4.8 %all-gather.9.cloned.1.call-done = bf16[256,2048]{1,0:T(8,128)(2,1)} async-done(((bf16[256,256]{1,0:T(8,128)(2,1)}), bf16[256,2048]{1,0:T(8,128)(2,1)}) %all-gather.9.cloned.1.call-update) | async-done | bytes 1048592 | tf_op jit(solution)/shard_map/all_gather | solution.py:148
  176.7 1.8 fusion.40
  180.6 7.1 %all-gather.1 = f32[512,1]{0,1:T(1,128)S(1)} all-gather(f32[128,1]{0,1:T(1,128)S(1)} %get-tuple-element.168), channel_id=3, replica_groups=mesh['sp'=4,'tp'=8] {'sp'}, dimensions={0}, use_global_device_ids=true | all-gather | bytes 2560 | tf_op jit(solution)/shard_map/all_gather | solution.py:14
  187.8 7.9 %all-gather.2 = f32[512,1]{0,1:T(1,128)S(1)} all-gather(f32[128,1]{0,1:T(1,128)S(1)} %get-tuple-element.167), channel_id=4, replica_groups=mesh['sp'=4,'tp'=8] {'sp'}, dimensions={0}, use_global_device_ids=true | all-gather | bytes 2560 | tf_op jit(solution)/shard_map/all_gather | solution.py:14
  195.7 1.4 convolution_convert_fusion
  197.5 0.2 fusion.43
  197.8 0.9 fusion.62
  199.0 0.9 fusion.59
  200.0 0.7 copy.155
  200.7 0.7 copy.156
  201.5 19.8 %reduce-scatter.5.cloned.1.call-done = bf16[512,128]{1,0:T(8,128)(2,1)} async-done(((bf16[2048,128]{1,0:T(8,128)(2,1)}), bf16[512,128]{1,0:T(8,128)(2,1)}) %reduce-scatter.5.cloned.1.call-update) | async-done | bytes 131088 | tf_op jit(solution)/shard_map/reduce_scatter | solution.py:220
  221.2 0.9 convert_bitcast_fusion.3
  222.2 0.8 copy.154
  (211 shorter events, 3.4 us)
Async XLA Ops:
  7.2 169.6 %copy-start = (bf16[128,2048]{1,0:T(8,128)(2,1)S(1)}, bf16[128,2048]{1,0:T(8,128)(2,1)}, u32[]{:S(2)}) copy-start(bf16[128,2048]{1,0:T(8,128)(2,1)} %param.24) | copy-start | bytes 1572868
  7.2 17.1 %copy-start.4 = (bf16[256,256]{1,0:T(8,128)(2,1)S(1)}, bf16[256,256]{1,0:T(8,128)(2,1)}, u32[]{:S(2)}) copy-start(bf16[256,256]{1,0:T(8,128)(2,1)} %param.17) | copy-start | bytes 393220
  7.2 17.1 %copy-start.17 = (f32[256,2]{0,1:T(2,128)S(1)}, f32[256,2]{0,1:T(2,128)}, u32[]{:S(2)}) copy-start(f32[256,2]{0,1:T(2,128)} %param.20) | copy-start | bytes 6148
  7.2 50.4 %all-gather.11.cloned.1.call-start = ((), (), s32[]{:S(2)}) async-start(), calls=%async_computation.9 | async-start | bytes 2949120 | tf_op jit(solution)/shard_map/all_gather | solution.py:122
  24.2 69.0 %all-gather.7.cloned.1.call-start = ((), (), s32[]{:S(2)}) async-start(), calls=%async_computation.5 | async-start | bytes 2949120 | tf_op jit(solution)/shard_map/all_gather | solution.py:126
  34.1 110.6 %reduce-scatter.3.cloned.1.call-start = ((), (), s32[]{:S(2)}) async-start(), calls=%async_computation.6 | async-start | bytes 2949120 | tf_op jit(solution)/shard_map/reduce_scatter | solution.py:135
  60.8 2.5 %copy-start.12 = (bf16[1,2048,896]{2,1,0:T(8,128)(2,1)S(1)}, bf16[1,2048,896]{2,1,0:T(8,128)(2,1)}, u32[]{:S(2)}) copy-start(bf16[1,2048,896]{2,1,0:T(8,128)(2,1)} %param.21) | copy-start | bytes 11010052
  61.7 5.9 %copy-start.1 = (bf16[80,8,8,256]{3,1,2,0:T(8,128)(2,1)}, bf16[80,8,8,256]{3,1,2,0:T(8,128)(2,1)S(1)}, u32[]{:S(2)}) copy-start(bf16[80,8,8,256]{3,1,2,0:T(8,128)(2,1)S(1)} %copy.162) | copy-start | bytes 7864324
  63.4 4.3 %copy-start.14 = (bf16[1,2048,896]{2,1,0:T(8,128)(2,1)S(1)}, bf16[1,2048,896]{2,1,0:T(8,128)(2,1)}, u32[]{:S(2)}) copy-start(bf16[1,2048,896]{2,1,0:T(8,128)(2,1)} %param.22) | copy-start | bytes 11010052
  93.3 7.8 %copy-start.13 = (bf16[1,2048,896]{2,1,0:T(8,128)(2,1)S(1)}, bf16[1,2048,896]{2,1,0:T(8,128)(2,1)}, u32[]{:S(2)}) copy-start(bf16[1,2048,896]{2,1,0:T(8,128)(2,1)} %param.21) | copy-start | bytes 11010052
  101.1 3.0 %copy-start.18 = (bf16[640,896]{1,0:T(8,128)(2,1)}, bf16[640,896]{1,0:T(8,128)(2,1)S(1)}, u32[]{:S(2)}) copy-start(bf16[640,896]{1,0:T(8,128)(2,1)S(1)} %get-tuple-element.164) | copy-start | bytes 3440644
  101.1 3.0 %copy-start.22 = (bf16[640,896]{1,0:T(8,128)(2,1)}, bf16[640,896]{1,0:T(8,128)(2,1)S(1)}, u32[]{:S(2)}) copy-start(bf16[640,896]{1,0:T(8,128)(2,1)S(1)} %get-tuple-element.163) | copy-start | bytes 3440644
  101.1 2.9 %copy-start.15 = (bf16[1,2048,896]{2,1,0:T(8,128)(2,1)S(1)}, bf16[1,2048,896]{2,1,0:T(8,128)(2,1)}, u32[]{:S(2)}) copy-start(bf16[1,2048,896]{2,1,0:T(8,128)(2,1)} %param.22) | copy-start | bytes 11010052
  108.4 0.8 copy-start.9
  108.4 41.7 %copy-start.10 = (bf16[128,256]{1,0:T(8,128)(2,1)S(1)}, bf16[128,256]{1,0:T(8,128)(2,1)}, u32[]{:S(2)}) copy-start(bf16[128,256]{1,0:T(8,128)(2,1)} %param.27) | copy-start | bytes 196612
  108.4 41.8 %copy-start.11 = (bf16[128,256]{1,0:T(8,128)(2,1)S(1)}, bf16[128,256]{1,0:T(8,128)(2,1)}, u32[]{:S(2)}) copy-start(bf16[128,256]{1,0:T(8,128)(2,1)} %param.26) | copy-start | bytes 196612
  108.4 42.5 %copy-start.7 = (f32[128,256]{1,0:T(8,128)S(1)}, f32[128,256]{1,0:T(8,128)}, u32[]{:S(2)}) copy-start(f32[128,256]{1,0:T(8,128)} %param.31) | copy-start | bytes 393220
  144.7 9.2 %all-to-all-start.2 = ((bf16[4,160,256]{2,1,0:T(8,128)(2,1)}), bf16[4,160,256]{2,1,0:T(8,128)(2,1)S(1)}, u32[]{:S(2)}, u32[]{:S(2)}) async-start(bf16[4,160,256]{2,1,0:T(8,128)(2,1)} %reduce-scatter.3.cloned.1.call-done), calls=%async_computation.3 | async-start | bytes 655360 | tf_op jit(solution)/shard_map/all_to_all | solution.py:141
  148.4 28.4 %all-gather.9.cloned.1.call-start = ((), (), s32[]{:S(2)}) async-start(), calls=%async_computation.7 | async-start | bytes 1179648 | tf_op jit(solution)/shard_map/all_gather | solution.py:148
  154.9 7.5 %copy-start.2 = (bf16[80,8,8,256]{3,1,2,0:T(8,128)(2,1)S(1)}, bf16[80,8,8,256]{3,1,2,0:T(8,128)(2,1)}, u32[]{:S(2)}) copy-start(bf16[80,8,8,256]{3,1,2,0:T(8,128)(2,1)} %copy-done.1) | copy-start | bytes 7864324
  154.9 66.3 %reduce-scatter.5.cloned.1.call-start = ((), (), s32[]{:S(2)}) async-start(), calls=%async_computation.8 | async-start | bytes 655360 | tf_op jit(solution)/shard_map/reduce_scatter | solution.py:220
  155.0 7.4 %copy-start.19 = (bf16[640,896]{1,0:T(8,128)(2,1)S(1)}, bf16[640,896]{1,0:T(8,128)(2,1)}, u32[]{:S(2)}) copy-start(bf16[640,896]{1,0:T(8,128)(2,1)} %copy-done.18) | copy-start | bytes 3440644
  162.4 4.9 %copy-start.16 = (bf16[4,160,2048]{2,1,0:T(8,128)(2,1)S(1)}, bf16[4,160,2048]{2,1,0:T(8,128)(2,1)}, u32[]{:S(2)}) copy-start(bf16[4,160,2048]{2,1,0:T(8,128)(2,1)} %all-gather.7.cloned.1.call-done) | copy-start | bytes 7864324
  162.4 4.9 %copy-start.20 = (f32[640,896]{1,0:T(8,128)S(1)}, f32[640,896]{1,0:T(8,128)}, u32[]{:S(2)}) copy-start(f32[640,896]{1,0:T(8,128)} %fusion.3) | copy-start | bytes 6881284
  162.4 4.9 %copy-start.21 = (f32[640,896]{1,0:T(8,128)S(1)}, f32[640,896]{1,0:T(8,128)}, u32[]{:S(2)}) copy-start(f32[640,896]{1,0:T(8,128)} %fusion.7) | copy-start | bytes 6881284
  167.3 9.5 %copy-start.5 = (f32[128,256]{0,1:T(8,128)S(1)}, f32[128,256]{0,1:T(8,128)}, u32[]{:S(2)}) copy-start(f32[128,256]{0,1:T(8,128)} %copy.136) | copy-start | bytes 393220
  167.3 9.5 %copy-start.6 = (bf16[128,256]{0,1:T(8,128)(2,1)S(1)}, bf16[128,256]{0,1:T(8,128)(2,1)}, u32[]{:S(2)}) copy-start(bf16[128,256]{0,1:T(8,128)(2,1)} %copy.134) | copy-start | bytes 196612
  167.3 9.5 %copy-start.8 = (f32[128,256]{0,1:T(8,128)S(1)}, f32[128,256]{0,1:T(8,128)}, u32[]{:S(2)}) copy-start(f32[128,256]{0,1:T(8,128)} %copy.137) | copy-start | bytes 393220
  178.9 16.9 %copy-start.3 = (bf16[256,2048]{1,0:T(8,128)(2,1)S(1)}, bf16[256,2048]{1,0:T(8,128)(2,1)}, u32[]{:S(2)}) copy-start(bf16[256,2048]{1,0:T(8,128)(2,1)} %all-gather.9.cloned.1.call-done) | copy-start | bytes 3145732
Sparse Core Ops, SparseCore 0:
  24.3 33.2 all-gather.10
  59.2 34.0 all-gather.6
  108.6 36.1 reduce-scatter.2
  155.0 21.6 all-gather.8
  197.3 23.9 reduce-scatter.4
